TPU v7x, 256 devices: a whole 4x4x8 slice. The times are simulated.
256 devices in a mesh: sp: 64 (over z, x, core), tp: 4 (over y).
Axes of the slice: x: 4, y: 4, z: 8, core: 2. Of those that a mesh axis runs over, the one named last changes fastest.
Arguments:
- hidden_in: bfloat16 [16384, 2048], P('sp'), may hold values from -6 to 6
- cotangent: bfloat16 [16384, 2048], P('sp'), may hold values from -16 to 16
- routes: int32 [16384, 2], P('sp'), may hold values from 0 to 63, all different within a row; in each aligned block of 256 rows (0 to 255, 256 to 511, ...) at most 12 rows name the same one
- routing_weights: float32 [16384, 2], P('sp'), may hold values from 0.1 to 1
- w_gate: bfloat16 [64, 2048, 1024], P('sp', None, 'tp'), may hold values from -0.125 to 0.125
- w_up: bfloat16 [64, 2048, 1024], P('sp', None, 'tp'), may hold values from -0.125 to 0.125
- w_down: bfloat16 [64, 1024, 2048], P('sp', 'tp'), may hold values from -0.1875 to 0.1875
- b_gate: bfloat16 [16384, 1024], P('sp', 'tp'), may hold values from -6 to 6
- c_gate: bfloat16 [16384, 1024], P('sp', 'tp'), may hold values from -6 to 6
- x_in: bfloat16 [16384, 1024], P('sp', 'tp'), may hold values from -6 to 6
- taps: bfloat16 [3, 1024], P(None, 'tp'), may hold values from -3 to 3
- w_out: bfloat16 [2048, 1024], P(None, 'tp'), may hold values from -0.1875 to 0.1875
Outputs:
- grad_gate: bfloat16 [64, 2048, 1024], P('sp', None, 'tp')
- grad_up: bfloat16 [64, 2048, 1024], P('sp', None, 'tp')
- grad_down: bfloat16 [64, 1024, 2048], P('sp', 'tp')
- out_proj_grad: float32 [2048, 1024], P('sp', 'tp')
- residual_grad: bfloat16 [16384, 2048], P('sp', 'tp')
- grad_b: bfloat16 [16384, 1024], P('sp', 'tp')
- grad_c: bfloat16 [16384, 1024], P('sp', 'tp')
- grad_x: bfloat16 [16384, 1024], P('sp', 'tp')
Inputs may be any that keep to these rules, and one draw needn't show every extreme that they name: `routes`: each row names 2 different experts. Among the rows of one index of sp no expert is named more than 12 times, a bound that some block reaches in some of them.
All inputs are finite; a program needn't handle non-finite values.
Results may differ from a plain program's by a relative error of at most 0.01.
Values may be sent and summed in bfloat16 or wider, within the bound.
No kernel may reach another device: no remote copies, remote signals or barrier semaphores. Data moves between devices by JAX's collectives and lax.ppermute only.
A program may use at most 64 MiB of HBM per device.

v0:
```python
import jax
import jax.numpy as jnp
from jax import lax
from jax.sharding import PartitionSpec as P


def in_one_piece(arrays, axis, split_dim, concat_dim, along):
    widths = [a.shape[along] for a in arrays]
    both = jnp.concatenate(arrays, axis=along)
    whole = lax.all_to_all(both, axis, split_axis=split_dim, concat_axis=concat_dim, tiled=True)
    return tuple(jnp.split(whole, [sum(widths[:k]) for k in range(1, len(widths))], axis=along))


def sent_together(arrays, axis, dim, along):
    ends, at = ([], 0)
    for a in arrays[:-1]:
        at += a.shape[along]
        ends.append(at)
    both = jnp.concatenate(arrays, axis=along)
    return tuple(jnp.split(lax.all_gather(both, axis, axis=dim, tiled=True), ends, axis=along))


def cut_along(x, dim, devices):
    before, after = (x.shape[:dim], x.shape[dim + 1 :])
    return jnp.moveaxis(x.reshape(*before, devices, -1, *after), dim, 0)


def summed_on_arrival(x, axis, dim):
    blocks = cut_along(x, dim, lax.axis_size(axis))
    arrived = lax.all_to_all(blocks, axis, split_axis=0, concat_axis=0, tiled=True)
    return arrived.astype(jnp.float32).sum(axis=0)


def laid_out(blocks, dim):
    lengths = list(blocks.shape[1:])
    lengths[dim] *= blocks.shape[0]
    return jnp.moveaxis(blocks, 0, dim).reshape(lengths)


def copy_for_each(x, axis):
    copies = jnp.broadcast_to(x, (lax.axis_size(axis), *x.shape))
    return lax.all_to_all(copies, axis, split_axis=0, concat_axis=0, tiled=True)


def gathered_copies(x, axis, dim):
    return laid_out(copy_for_each(x, axis), dim)


def from_behind(x, axis, by):
    devices = lax.axis_size(axis)
    pairs = [(i, i + by) for i in range(devices) if 0 <= i + by < devices]
    return lax.ppermute(x, axis, pairs)


def per_device(
    hidden_in,
    cotangent,
    routes,
    routing_weights,
    w_gate,
    w_up,
    w_down,
    b_gate,
    c_gate,
    x_in,
    taps,
    w_out,
):
    tok_rows, model_width = hidden_in.shape
    top_k = routes.shape[1]
    local_experts = w_gate.shape[0]
    sp_size = lax.axis_size("sp")
    tp_size = lax.axis_size("tp")
    experts = local_experts * sp_size
    capacity = 3 * tok_rows * top_k // (2 * experts)
    slot_count = tok_rows * top_k
    feature_share = model_width // tp_size
    share_offset = lax.axis_index("tp") * feature_share
    flat_ids = routes.reshape(-1)
    onehot = (flat_ids[:, None] == jnp.arange(experts, dtype=jnp.int32)[None, :]).astype(jnp.int32)
    before = jnp.cumsum(onehot, axis=0) - onehot
    position = jnp.sum(before * onehot, axis=1)
    target = flat_ids * capacity + position
    source = (
        jnp.full((experts * capacity,), slot_count, jnp.int32)
        .at[target]
        .set(jnp.arange(slot_count, dtype=jnp.int32))
    )
    filled = source < slot_count
    clipped = jnp.minimum(source, slot_count - 1)
    token_of = clipped // top_k
    weight_of = jnp.where(filled, routing_weights.reshape(-1)[clipped], 0.0)
    rows_src = lax.dynamic_slice_in_dim(hidden_in, share_offset, feature_share, 1)
    cot_src = lax.dynamic_slice_in_dim(cotangent, share_offset, feature_share, 1)
    send_rows = jnp.where(filled[:, None], rows_src[token_of], jnp.zeros((), jnp.bfloat16))
    send_rows = send_rows.reshape(experts, capacity, -1)
    send_cot = (weight_of[:, None] * cot_src[token_of].astype(jnp.float32)).astype(jnp.bfloat16)
    send_cot = send_cot.reshape(experts, capacity, -1)
    part_rows, part_cot = in_one_piece((send_rows, send_cot), "sp", 0, 1, 2)
    rows_h, rows_s = sent_together((part_rows, part_cot), "tp", 2, 0)
    pre_gate = jnp.einsum("erd,edf->erf", rows_h, w_gate, preferred_element_type=jnp.float32)
    pre_up = jnp.einsum("erd,edf->erf", rows_h, w_up, preferred_element_type=jnp.float32)
    sigma = jax.nn.sigmoid(pre_gate)
    silu_gate = pre_gate * sigma
    hid = (silu_gate * pre_up).astype(jnp.bfloat16)
    d_hid = jnp.einsum("erd,efd->erf", rows_s, w_down, preferred_element_type=jnp.float32)
    d_up = (d_hid * silu_gate).astype(jnp.bfloat16)
    d_pre = (d_hid * pre_up * sigma * (1.0 + pre_gate * (1.0 - sigma))).astype(jnp.bfloat16)
    grad_down = jnp.einsum("erf,erd->efd", hid, rows_s, preferred_element_type=jnp.float32).astype(
        jnp.bfloat16
    )
    grad_gate = jnp.einsum(
        "erd,erf->edf", rows_h, d_pre, preferred_element_type=jnp.float32
    ).astype(jnp.bfloat16)
    grad_up = jnp.einsum("erd,erf->edf", rows_h, d_up, preferred_element_type=jnp.float32).astype(
        jnp.bfloat16
    )
    partial_grad = jnp.einsum("erf,edf->erd", d_pre, w_gate, preferred_element_type=jnp.float32)
    partial_grad = partial_grad + jnp.einsum(
        "erf,edf->erd", d_up, w_up, preferred_element_type=jnp.float32
    )
    partial_low = partial_grad.astype(jnp.bfloat16)
    shared_rows = summed_on_arrival(partial_low, "tp", 2).astype(jnp.bfloat16)
    back = lax.all_to_all(shared_rows, "sp", split_axis=1, concat_axis=0, tiled=True)
    back_flat = back.reshape(experts * capacity, feature_share)
    per_token = back_flat[target].astype(jnp.float32).reshape(tok_rows, top_k, feature_share)
    own_cot = lax.dynamic_slice_in_dim(cotangent, share_offset, feature_share, 1).astype(
        jnp.float32
    )
    residual_grad = (own_cot + jnp.sum(per_token, axis=1)).astype(jnp.bfloat16)
    full_grad = gathered_copies(residual_grad, "tp", 1)
    taps_f = taps.astype(jnp.float32)
    gated = c_gate.astype(jnp.float32) * x_in.astype(jnp.float32)
    earlier = from_behind(gated[tok_rows - 2 :], "sp", 1)
    padded = jnp.concatenate([earlier, gated], axis=0)
    conv = (
        taps_f[0] * padded[0:tok_rows]
        + taps_f[1] * padded[1 : tok_rows + 1]
        + taps_f[2] * padded[2 : tok_rows + 2]
    )
    b_f = b_gate.astype(jnp.float32)
    y_short = (b_f * conv).astype(jnp.bfloat16)
    d_y = jnp.dot(full_grad, w_out, preferred_element_type=jnp.float32)
    grad_b = (d_y * conv).astype(jnp.bfloat16)
    d_conv = b_f * d_y
    following = from_behind(d_conv[0:2], "sp", -1)
    later = jnp.concatenate([d_conv, following], axis=0)
    d_v = (
        taps_f[2] * later[0:tok_rows]
        + taps_f[1] * later[1 : tok_rows + 1]
        + taps_f[0] * later[2 : tok_rows + 2]
    )
    grad_c = (d_v * x_in.astype(jnp.float32)).astype(jnp.bfloat16)
    grad_x = (d_v * c_gate.astype(jnp.float32)).astype(jnp.bfloat16)
    out_proj_grad = summed_on_arrival(
        jnp.einsum("td,tc->dc", full_grad, y_short, preferred_element_type=jnp.float32).astype(
            jnp.bfloat16
        ),
        "sp",
        0,
    )
    return (grad_gate, grad_up, grad_down, out_proj_grad, residual_grad, grad_b, grad_c, grad_x)


def solution(mesh):
    return jax.shard_map(
        per_device,
        mesh=mesh,
        in_specs=(
            P("sp", None),
            P("sp", None),
            P("sp", None),
            P("sp", None),
            P("sp", None, "tp"),
            P("sp", None, "tp"),
            P("sp", "tp", None),
            P("sp", "tp"),
            P("sp", "tp"),
            P("sp", "tp"),
            P(None, "tp"),
            P(None, "tp"),
        ),
        out_specs=(
            P("sp", None, "tp"),
            P("sp", None, "tp"),
            P("sp", "tp", None),
            P("sp", "tp"),
            P("sp", "tp"),
            P("sp", "tp"),
            P("sp", "tp"),
            P("sp", "tp"),
        ),
        check_vma=False,
    )
```

profile of v0, /device:TPU:1, one launch (start us, length us, event | category | flops | bytes accessed | tf_op | source)
XLA Modules:
  0.0 338.7 jit_solution(15847824969472595862)
XLA Ops:
  7.2 0.8 broadcast_multiply_fusion
  8.0 0.8 copy.34
  8.8 0.1 eq.25
  9.0 0.1 eq.29
  9.2 0.1 mul.129
  9.4 1.2 reduce-window.6
  10.6 0.2 slice_reduce_fusion
  11.0 2.4 scatter_custom_fusion
  13.5 1.0 constant_dynamic-slice_fusion
  14.5 3.3 gather_fusion.2
  17.8 1.2 reshape.179
  19.2 0.1 reshape.169
  19.4 5.0 %gather_fusion.1 = f32[768]{0:T(1024)S(1)} fusion(f32[512]{0:T(512)S(1)} %reshape.169, s32[1024]{0:T(1024)S(1)} %get-tuple-element.24), kind=kCustom, calls=%fused_computation.1 | custom fusion | bytes 9216 | tf_op jit(solution)/shard_map/gather | solution.py:92
  24.5 1.0 constant_dynamic-slice_fusion.1
  25.5 3.3 gather_fusion
  28.8 2.1 gather.15
  31.0 0.2 multiply_convert_fusion
  31.2 1.0 copy-done.2
  32.2 0.2 broadcast_select_fusion
  32.4 0.3 pad_maximum_fusion
  32.8 62.5 %all_to_all.36 = bf16[64,12,1024]{2,1,0:T(8,128)(2,1)S(1)} all-to-all(bf16[64,12,1024]{2,1,0:T(8,128)(2,1)S(1)} %pad_maximum_fusion), channel_id=1, replica_groups=mesh['sp'=64,'tp'=4] {'sp'}, dimensions={0} | all-to-all | bytes 3145728 | tf_op jit(solution)/shard_map/all_to_all | solution.py:10
  95.2 1.3 all_to_all.26
  96.6 1.5 fusion.41
  98.1 1.3 pad_maximum_fusion.1
  99.4 66.0 %all-gather.2.cloned.1.call-done = bf16[2,768,2048]{2,1,0:T(8,128)(2,1)} async-done(((bf16[2,768,512]{2,1,0:T(8,128)(2,1)}), bf16[2,768,2048]{2,1,0:T(8,128)(2,1)}) %all-gather.2.cloned.1.call-update) | async-done | bytes 6291472 | tf_op jit(solution)/shard_map/all_gather | solution.py:20
  165.3 3.0 fusion.6
  168.4 0.7 copy-done.14
  169.1 1.0 fusion.7
  170.1 0.5 copy-done.15
  170.6 1.2 multiply_convert_fusion.2
  171.8 1.0 fusion.8
  172.8 2.8 add_convert_fusion
  175.6 4.8 %reshape.175 = bf16[1,768,4,512]{3,2,1,0:T(4,128)(2,1)S(1)} reshape(bf16[768,2048]{1,0:T(8,128)(2,1)} %add_convert_fusion) | data formatting | bytes 6291456 | tf_op jit(solution)/shard_map/reshape | solution.py:25
  180.4 0.6 copy.47
  181.1 39.7 %all_to_all.37 = bf16[4,1,768,512]{3,2,1,0:T(8,128)(2,1)S(1)} all-to-all(bf16[4,1,768,512]{3,2,1,0:T(8,128)(2,1)S(1)} %bitcast.84), channel_id=1, replica_groups=mesh['sp'=64,'tp'=4] {'tp'}, dimensions={0} | all-to-all | bytes 6291456 | tf_op jit(solution)/shard_map/all_to_all | solution.py:30
  220.8 1.6 reduce_sum.45
  222.4 2.3 copy.49
  224.7 0.5 broadcast.112
  225.2 5.4 %reduce.4 = bf16[768,512]{1,0:T(8,128)(2,1)S(1)} reduce(bf16[768,1,512]{2,1,0:T(2,128)(2,1)S(1)} %bitcast.87, bf16[]{:T(256)} %broadcast.112), dimensions={1}, to_apply=%bitcast.82.reduce_sub_computation | reduce | bytes 1572866
  230.7 1.2 reshape.227
  231.9 12.0 %all-to-all-start.2 = ((bf16[64,2,3072]{2,1,0:T(2,128)(2,1)}), bf16[64,2,3072]{2,1,0:T(2,128)(2,1)S(1)}, u32[]{:S(2)}, u32[]{:S(2)}) async-start(bf16[64,2,3072]{2,1,0:T(2,128)(2,1)} %reshape.227), calls=%async_computation.2 | async-start | bytes 1572864 | tf_op jit(solution)/shard_map/all_to_all | solution.py:124
  243.9 23.0 %all-to-all-done.2 = bf16[64,2,3072]{2,1,0:T(2,128)(2,1)S(1)} async-done(((bf16[64,2,3072]{2,1,0:T(2,128)(2,1)}), bf16[64,2,3072]{2,1,0:T(2,128)(2,1)S(1)}, u32[]{:S(2)}, u32[]{:S(2)}) %all-to-all-start.2) | async-done | bytes 786464 | tf_op jit(solution)/shard_map/all_to_all | solution.py:124
  266.9 0.6 reshape.228
  267.5 0.2 copy.48
  267.7 2.0 gather_fusion.3
  269.7 0.7 reshape.180
  270.4 1.2 reduce_sum.47
  271.6 1.0 add_convert_fusion.1
  272.8 1.0 broadcast_in_dim.39
  273.9 3.8 %all-to-all-start.3 = ((bf16[4,256,512]{1,2,0:T(8,128)(2,1)}), bf16[4,256,512]{1,2,0:T(8,128)(2,1)S(1)}, u32[]{:S(2)}, u32[]{:S(2)}) async-start(bf16[4,256,512]{1,2,0:T(8,128)(2,1)} %broadcast_in_dim.39), calls=%async_computation.3 | async-start | bytes 2097152 | tf_op jit(solution)/shard_map/all_to_all | solution.py:42
  277.7 3.7 %collective-permute-start = (f32[2,256]{1,0:T(2,128)S(1)}, f32[2,256]{1,0:T(2,128)S(1)}, u32[]{:S(2)}, u32[]{:S(2)}) collective-permute-start(f32[2,256]{1,0:T(2,128)S(1)} %slice.57), channel_id=1, source_target_pairs={{0,4},{4,8},{8,12},{12,16},{16,20},{20,24},{24,28},{28,32},{32,36}... | collective-permute-start | bytes 6152 | tf_op jit(solution)/shard_map/ppermute | solution.py:52
  281.4 0.7 collective-permute-done
  282.1 9.7 %all-to-all-done.3 = bf16[4,256,512]{1,2,0:T(8,128)(2,1)S(1)} async-done(((bf16[4,256,512]{1,2,0:T(8,128)(2,1)}), bf16[4,256,512]{1,2,0:T(8,128)(2,1)S(1)}, u32[]{:S(2)}, u32[]{:S(2)}) %all-to-all-start.3) | async-done | bytes 1048608 | tf_op jit(solution)/shard_map/all_to_all | solution.py:42
  291.9 2.0 multiply_convert_fusion.5
  293.9 2.3 convolution_convert_fusion
  296.2 6.6 %all-to-all-start.4 = ((bf16[64,32,256]{2,1,0:T(8,128)(2,1)}), bf16[64,32,256]{2,1,0:T(8,128)(2,1)S(1)}, u32[]{:S(2)}, u32[]{:S(2)}) async-start(bf16[64,32,256]{2,1,0:T(8,128)(2,1)} %bitcast.18), calls=%async_computation.4 | async-start | bytes 2097152 | tf_op jit(solution)/shard_map/all_to_all | solution.py:30
  302.9 4.0 %fusion.3 = bf16[1,2048,256]{2,1,0:T(8,128)(2,1)} fusion(bf16[768,256]{1,0:T(8,128)(2,1)S(1)} %get-tuple-element.15, bf16[2,768,2048]{2,1,0:T(8,128)(2,1)} %all-gather.2.cloned.1.call-done), kind=kOutput, calls=%fused_computation.15 | convolution fusion | flops 805830656 | bytes 4587520 | tf_op jit(solution)/shard_map/erd,erf->edf/dot_general | solution.py:112
  306.9 4.0 %fusion.5 = bf16[1,256,2048]{2,1,0:T(8,128)(2,1)} fusion(bf16[2,768,2048]{2,1,0:T(8,128)(2,1)} %all-gather.2.cloned.1.call-done, f32[768,256]{1,0:T(8,128)S(1)} %copy-done.19, f32[768,256]{1,0:T(8,128)S(1)} %copy-done.17), kind=kOutput, calls=%fused_computation.17 | convolution fusion | flops 807010304 | bytes 5767168 | tf_op jit(solution)/shard_map/erf,erd->efd/dot_general | solution.py:109
  310.9 2.5 collective-permute-start.1
  313.4 4.0 %fusion.4 = bf16[1,2048,256]{2,1,0:T(8,128)(2,1)} fusion(bf16[768,256]{1,0:T(8,128)(2,1)S(1)} %copy-done.11, bf16[2,768,2048]{2,1,0:T(8,128)(2,1)} %all-gather.2.cloned.1.call-done), kind=kOutput, calls=%fused_computation.16 | convolution fusion | flops 805830656 | bytes 4587520 | tf_op jit(solution)/shard_map/erd,erf->edf/dot_general | solution.py:115
  317.4 0.8 fusion.24
  318.2 0.7 fusion.25
  318.9 12.2 %all-to-all-done.4 = bf16[64,32,256]{2,1,0:T(8,128)(2,1)S(1)} async-done(((bf16[64,32,256]{2,1,0:T(8,128)(2,1)}), bf16[64,32,256]{2,1,0:T(8,128)(2,1)S(1)}, u32[]{:S(2)}, u32[]{:S(2)}) %all-to-all-start.4) | async-done | bytes 1048608 | tf_op jit(solution)/shard_map/all_to_all | solution.py:30
  331.0 0.8 convert_reduce_fusion
  (59 shorter events, 1.0 us)
Async XLA Ops:
  7.2 158.2 %copy-start = (bf16[1,2048,256]{2,1,0:T(8,128)(2,1)S(1)}, bf16[1,2048,256]{2,1,0:T(8,128)(2,1)}, u32[]{:S(2)}) copy-start(bf16[1,2048,256]{2,1,0:T(8,128)(2,1)} %param.16) | copy-start | bytes 3145732
  7.2 158.2 %all-gather.2.cloned.1.call-start = ((), (), s32[]{:S(2)}) async-start(), calls=%async_computation.5 | async-start | bytes 7864320 | tf_op jit(solution)/shard_map/all_gather | solution.py:20
  14.5 4.6 %copy-start.13 = (f32[256,2]{0,1:T(2,128)S(1)}, f32[256,2]{0,1:T(2,128)}, u32[]{:S(2)}) copy-start(f32[256,2]{0,1:T(2,128)} %param.15) | copy-start | bytes 6148
  31.0 1.2 copy-start.2
  99.4 69.0 %copy-start.5 = (bf16[1,2048,256]{2,1,0:T(8,128)(2,1)S(1)}, bf16[1,2048,256]{2,1,0:T(8,128)(2,1)}, u32[]{:S(2)}) copy-start(bf16[1,2048,256]{2,1,0:T(8,128)(2,1)} %param.17) | copy-start | bytes 3145732
  165.3 3.7 %copy-start.14 = (bf16[2,768,2048]{2,1,0:T(8,128)(2,1)S(1)}, bf16[2,768,2048]{2,1,0:T(8,128)(2,1)}, u32[]{:S(2)}) copy-start(bf16[2,768,2048]{2,1,0:T(8,128)(2,1)} %all-gather.2.cloned.1.call-done) | copy-start | bytes 18874372
  169.1 1.0 copy-start.16
  169.1 1.5 copy-start.15
  170.6 1.2 copy-start.18
  171.8 1.0 copy-start.10
  231.9 35.0 %all-to-all-start.2 = ((bf16[64,2,3072]{2,1,0:T(2,128)(2,1)}), bf16[64,2,3072]{2,1,0:T(2,128)(2,1)S(1)}, u32[]{:S(2)}, u32[]{:S(2)}) async-start(bf16[64,2,3072]{2,1,0:T(2,128)(2,1)} %reshape.227), calls=%async_computation.2 | async-start | bytes 1572864 | tf_op jit(solution)/shard_map/all_to_all | solution.py:124
  270.3 7.3 %copy-start.6 = (bf16[256,256]{1,0:T(8,128)(2,1)S(1)}, bf16[256,256]{1,0:T(8,128)(2,1)}, u32[]{:S(2)}) copy-start(bf16[256,256]{1,0:T(8,128)(2,1)} %param.20) | copy-start | bytes 393220
  270.4 7.3 %copy-start.8 = (bf16[256,256]{1,0:T(8,128)(2,1)S(1)}, bf16[256,256]{1,0:T(8,128)(2,1)}, u32[]{:S(2)}) copy-start(bf16[256,256]{1,0:T(8,128)(2,1)} %param.21) | copy-start | bytes 393220
  271.6 9.8 %copy-start.12 = (bf16[3,256]{1,0:T(4,128)(2,1)S(1)}, bf16[3,256]{1,0:T(4,128)(2,1)}, u32[]{:S(2)}) copy-start(bf16[3,256]{1,0:T(4,128)(2,1)} %param.22) | copy-start | bytes 4612
  272.7 21.2 %copy-start.4 = (bf16[256,512]{1,0:T(8,128)(2,1)}, bf16[256,512]{1,0:T(8,128)(2,1)S(1)}, u32[]{:S(2)}) copy-start(bf16[256,512]{1,0:T(8,128)(2,1)S(1)} %add_convert_fusion.1) | copy-start | bytes 786436
  272.7 19.2 %copy-start.3 = (bf16[2048,256]{1,0:T(8,128)(2,1)S(1)}, bf16[2048,256]{1,0:T(8,128)(2,1)}, u32[]{:S(2)}) copy-start(bf16[2048,256]{1,0:T(8,128)(2,1)} %param.23) | copy-start | bytes 3145732
  273.9 18.0 %all-to-all-start.3 = ((bf16[4,256,512]{1,2,0:T(8,128)(2,1)}), bf16[4,256,512]{1,2,0:T(8,128)(2,1)S(1)}, u32[]{:S(2)}, u32[]{:S(2)}) async-start(bf16[4,256,512]{1,2,0:T(8,128)(2,1)} %broadcast_in_dim.39), calls=%async_computation.3 | async-start | bytes 2097152 | tf_op jit(solution)/shard_map/all_to_all | solution.py:42
  277.7 4.4 %collective-permute-start = (f32[2,256]{1,0:T(2,128)S(1)}, f32[2,256]{1,0:T(2,128)S(1)}, u32[]{:S(2)}, u32[]{:S(2)}) collective-permute-start(f32[2,256]{1,0:T(2,128)S(1)} %slice.57), channel_id=1, source_target_pairs={{0,4},{4,8},{8,12},{12,16},{16,20},{20,24},{24,28},{28,32},{32,36}... | collective-permute-start | bytes 6152 | tf_op jit(solution)/shard_map/ppermute | solution.py:52
  296.2 34.8 %all-to-all-start.4 = ((bf16[64,32,256]{2,1,0:T(8,128)(2,1)}), bf16[64,32,256]{2,1,0:T(8,128)(2,1)S(1)}, u32[]{:S(2)}, u32[]{:S(2)}) async-start(bf16[64,32,256]{2,1,0:T(8,128)(2,1)} %bitcast.18), calls=%async_computation.4 | async-start | bytes 2097152 | tf_op jit(solution)/shard_map/all_to_all | solution.py:30
  302.9 4.0 %copy-start.17 = (f32[768,256]{1,0:T(8,128)S(1)}, f32[768,256]{1,0:T(8,128)}, u32[]{:S(2)}) copy-start(f32[768,256]{1,0:T(8,128)} %copy-done.16) | copy-start | bytes 2359300
  302.9 4.0 %copy-start.19 = (f32[768,256]{1,0:T(8,128)S(1)}, f32[768,256]{1,0:T(8,128)}, u32[]{:S(2)}) copy-start(f32[768,256]{1,0:T(8,128)} %copy-done.18) | copy-start | bytes 2359300
  306.9 6.5 %copy-start.11 = (bf16[768,256]{1,0:T(8,128)(2,1)S(1)}, bf16[768,256]{1,0:T(8,128)(2,1)}, u32[]{:S(2)}) copy-start(bf16[768,256]{1,0:T(8,128)(2,1)} %copy-done.10) | copy-start | bytes 1179652
  310.9 6.5 %copy-start.7 = (bf16[256,256]{1,0:T(8,128)(2,1)S(1)}, bf16[256,256]{1,0:T(8,128)(2,1)}, u32[]{:S(2)}) copy-start(bf16[256,256]{1,0:T(8,128)(2,1)} %param.20) | copy-start | bytes 393220
  310.9 7.3 %copy-start.9 = (bf16[256,256]{1,0:T(8,128)(2,1)S(1)}, bf16[256,256]{1,0:T(8,128)(2,1)}, u32[]{:S(2)}) copy-start(bf16[256,256]{1,0:T(8,128)(2,1)} %param.21) | copy-start | bytes 393220
  310.9 6.5 %collective-permute-start.1 = (f32[2,256]{1,0:T(2,128)S(1)}, f32[2,256]{1,0:T(2,128)S(1)}, u32[]{:S(2)}, u32[]{:S(2)}) collective-permute-start(f32[2,256]{1,0:T(2,128)S(1)} %slice.62), channel_id=1, source_target_pairs={{4,0},{8,4},{12,8},{16,12},{20,16},{24,20},{28,24},{32,28},{36,32}... | collective-permute-start | bytes 6152 | tf_op jit(solution)/shard_map/ppermute | solution.py:52
  313.4 18.4 %copy-start.1 = (bf16[1,2048,256]{2,1,0:T(8,128)(2,1)S(1)}, bf16[1,2048,256]{2,1,0:T(8,128)(2,1)}, u32[]{:S(2)}) copy-start(bf16[1,2048,256]{2,1,0:T(8,128)(2,1)} %param.16) | copy-start | bytes 3145732
Sparse Core Ops, SparseCore 0:
  99.5 65.8 all-gather.1
where the time goes:
time: 340 us; the launch traced here: 339 us
  waiting for transfers between devices  112 us (33%)
  blocking collectives  102 us (30%)
  local copies, waits for them, and re-layouts  40.7 us (12%)
  starting transfers between devices  28.6 us (8%)
  matrix products  25.4 us (7%)
  other arithmetic  15.7 us (5%)
  between operations  14.6 us (4%)
    all_gather x1, waiting for transfers between devices, sent_together(): lax.all_gather(both, axis, axis=dim, tiled=True)  66 us
    all_to_all x1, blocking collectives, in_one_piece(): lax.all_to_all(both, axis, split_axis=split_dim, concat_axis=concat_dim,...  62.5 us
    all_to_all x1, blocking collectives, summed_on_arrival(): lax.all_to_all(blocks, axis, split_axis=0, concat_axis=0, tiled=True)  39.7 us
    all_to_all x1, waiting for transfers between devices, per_device(): lax.all_to_all(shared_rows, 'sp', split_axis=1, concat_axis=0, tiled=True)  23 us
    all_to_all x1, waiting for transfers between devices, summed_on_arrival(): lax.all_to_all(blocks, axis, split_axis=0, concat_axis=0, tiled=True)  12.2 us
    all_to_all x1, starting transfers between devices, per_device(): lax.all_to_all(shared_rows, 'sp', split_axis=1, concat_axis=0, tiled=True)  12 us
    all_to_all x1, waiting for transfers between devices, copy_for_each(): return lax.all_to_all(copies, axis, split_axis=0, concat_axis=0, tiled=True)  9.72 us
  transfers between devices with their start and end apart: 6, of which 5 were waited for; matrix products, arithmetic and copies ran while one was open for 4% of the time, Pallas kernels for 0%

commit v1 on v0

--- a/solution.py
+++ b/solution.py
@@ -121,7 +121,10 @@
     )
     partial_low = partial_grad.astype(jnp.bfloat16)
     shared_rows = summed_on_arrival(partial_low, "tp", 2).astype(jnp.bfloat16)
-    back = lax.all_to_all(shared_rows, "sp", split_axis=1, concat_axis=0, tiled=True)
+    back = jnp.concatenate(
+        lax.all_to_all(jnp.stack(jnp.split(shared_rows, lax.axis_size("sp"), axis=1)), "sp", 0, 0),
+        axis=0,
+    )
     back_flat = back.reshape(experts * capacity, feature_share)
     per_token = back_flat[target].astype(jnp.float32).reshape(tok_rows, top_k, feature_share)
     own_cot = lax.dynamic_slice_in_dim(cotangent, share_offset, feature_share, 1).astype(

time: 340 us -> 379 us (1.11)
  local copies, waits for them, and re-layouts: 40.7 us -> 78.2 us
  other arithmetic: 15.7 us -> 11.6 us
  waiting for transfers between devices: 112 us -> 116 us
    unnamed x46 -> x103, local copies, waits for them, and re-layouts: 5.82 us -> 41.6 us
    unnamed x1 -> x0, other arithmetic: 5.43 us -> none
    all_to_all x1, waiting for transfers between devices: 23 us -> 28.1 us  [per_device(): lax.all_to_all(jnp.stack(jnp.split(shared_rows, lax.axis_size('sp'), axis...]
where the time goes in v1:
time: 379 us; the launch traced here: 378 us
  waiting for transfers between devices  116 us (31%)
  blocking collectives  102 us (27%)
  local copies, waits for them, and re-layouts  78.2 us (21%)
  starting transfers between devices  29.5 us (8%)
  matrix products  25.7 us (7%)
  between operations  14.5 us (4%)
  other arithmetic  11.6 us (3%)
    all_gather x1, waiting for transfers between devices, sent_together(): lax.all_gather(both, axis, axis=dim, tiled=True)  66 us
    all_to_all x1, blocking collectives, in_one_piece(): lax.all_to_all(both, axis, split_axis=split_dim, concat_axis=concat_dim,...  62.5 us
    unnamed x103, local copies, waits for them, and re-layouts  41.6 us
    all_to_all x1, blocking collectives, summed_on_arrival(): lax.all_to_all(blocks, axis, split_axis=0, concat_axis=0, tiled=True)  40 us
    all_to_all x1, waiting for transfers between devices, per_device(): lax.all_to_all(jnp.stack(jnp.split(shared_rows, lax.axis_size('sp'), axis...  28.1 us
    all_to_all x1, waiting for transfers between devices, summed_on_arrival(): lax.all_to_all(blocks, axis, split_axis=0, concat_axis=0, tiled=True)  12.2 us
    all_to_all x1, starting transfers between devices, per_device(): lax.all_to_all(jnp.stack(jnp.split(shared_rows, lax.axis_size('sp'), axis...  11.9 us
    all_to_all x1, waiting for transfers between devices, copy_for_each(): return lax.all_to_all(copies, axis, split_axis=0, concat_axis=0, tiled=True)  9.07 us
  transfers between devices with their start and end apart: 6, of which 5 were waited for; matrix products, arithmetic and copies ran while one was open for 4% of the time, Pallas kernels for 0%

profile of v1, /device:TPU:1, one launch (start us, length us, event | category | flops | bytes accessed | tf_op | source)
XLA Modules:
  0.0 378.0 jit_solution(11988881768943939928)
XLA Ops:
  7.2 0.8 broadcast_multiply_fusion
  8.0 0.8 copy.153
  9.4 1.2 reduce-window.6
  11.0 2.4 scatter_custom_fusion
  13.5 1.0 constant_dynamic-slice_fusion
  14.5 3.3 gather_fusion.2
  17.8 1.2 reshape.171
  19.4 5.0 %gather_fusion.1 = f32[768]{0:T(1024)S(1)} fusion(f32[512]{0:T(512)S(1)} %reshape.162, s32[1024]{0:T(1024)S(1)} %get-tuple-element.24), kind=kCustom, calls=%fused_computation.1 | custom fusion | bytes 9216 | tf_op jit(solution)/shard_map/gather | solution.py:92
  24.5 1.0 constant_dynamic-slice_fusion.1
  25.5 3.3 gather_fusion
  28.8 2.1 gather.15
  31.2 1.0 copy-done.1
  32.8 62.5 %all_to_all.32 = bf16[64,12,1024]{2,1,0:T(8,128)(2,1)S(1)} all-to-all(bf16[64,12,1024]{2,1,0:T(8,128)(2,1)S(1)} %pad_maximum_fusion), channel_id=1, replica_groups=mesh['sp'=64,'tp'=4] {'sp'}, dimensions={0} | all-to-all | bytes 3145728 | tf_op jit(solution)/shard_map/all_to_all | solution.py:10
  95.2 1.3 all_to_all.22
  96.6 1.5 fusion.41
  98.1 1.3 pad_maximum_fusion.1
  99.4 66.0 %all-gather.2.cloned.1.call-done = bf16[2,768,2048]{2,1,0:T(8,128)(2,1)} async-done(((bf16[2,768,512]{2,1,0:T(8,128)(2,1)}), bf16[2,768,2048]{2,1,0:T(8,128)(2,1)}) %all-gather.2.cloned.1.call-update) | async-done | bytes 6291472 | tf_op jit(solution)/shard_map/all_gather | solution.py:20
  165.4 3.0 fusion.6
  168.4 0.7 copy-done.13
  169.1 1.0 fusion.7
  170.6 1.2 multiply_convert_fusion.2
  171.8 1.0 fusion.8
  172.9 2.8 add_convert_fusion
  175.6 6.2 %reshape.168 = bf16[1,768,4,512]{3,2,1,0:T(4,128)(2,1)} reshape(bf16[768,2048]{1,0:T(8,128)(2,1)} %add_convert_fusion) | data formatting | bytes 6291456 | tf_op jit(solution)/shard_map/reshape | solution.py:25
  181.8 2.5 copy.162
  184.3 40.0 %all_to_all.33 = bf16[4,1,768,512]{3,2,1,0:T(8,128)(2,1)} all-to-all(bf16[4,1,768,512]{3,2,1,0:T(8,128)(2,1)S(1)} %bitcast.332), channel_id=1, replica_groups=mesh['sp'=64,'tp'=4] {'tp'}, dimensions={0} | all-to-all | bytes 6291456 | tf_op jit(solution)/shard_map/all_to_all | solution.py:30
  224.3 2.8 reduce_sum.45
  227.7 0.6 constant_dynamic-update-slice_fusion.62
  228.9 0.6 constant_dynamic-update-slice_fusion.60
  230.2 0.6 constant_dynamic-update-slice_fusion.58
  231.4 0.6 constant_dynamic-update-slice_fusion.56
  232.6 0.6 constant_dynamic-update-slice_fusion.54
  233.8 0.6 constant_dynamic-update-slice_fusion.52
  235.0 0.6 constant_dynamic-update-slice_fusion.50
  236.3 0.6 constant_dynamic-update-slice_fusion.48
  237.5 0.6 constant_dynamic-update-slice_fusion.46
  241.1 0.6 constant_dynamic-update-slice_fusion.40
  244.8 0.6 constant_dynamic-update-slice_fusion.34
  248.5 0.6 constant_dynamic-update-slice_fusion.28
  257.0 0.6 constant_dynamic-update-slice_fusion.14
  260.6 0.6 constant_dynamic-update-slice_fusion.8
  264.3 0.6 constant_dynamic-update-slice_fusion.2
  266.1 11.9 %all-to-all-start.2 = ((bf16[64,1,12,512]{3,2,1,0:T(8,128)(2,1)}), bf16[64,1,12,512]{3,2,1,0:T(8,128)(2,1)S(1)}, u32[]{:S(2)}, u32[]{:S(2)}) async-start(bf16[64,1,12,512]{3,2,1,0:T(8,128)(2,1)} %constant_dynamic-update-slice_fusion), calls=%async_computation.2 | async-start | bytes 2097152 | tf_op jit(solution)/shard_map/all_to_all | solution.py:125
  278.1 28.1 %all-to-all-done.2 = bf16[64,1,12,512]{3,2,1,0:T(8,128)(2,1)S(1)} async-done(((bf16[64,1,12,512]{3,2,1,0:T(8,128)(2,1)}), bf16[64,1,12,512]{3,2,1,0:T(8,128)(2,1)S(1)}, u32[]{:S(2)}, u32[]{:S(2)}) %all-to-all-start.2) | async-done | bytes 786464 | tf_op jit(solution)/shard_map/all_to_all | solution.py:125
  306.4 2.0 gather_fusion.3
  308.4 0.7 reshape.172
  309.0 1.2 reduce_sum.47
  310.3 1.0 add_convert_fusion.1
  311.5 1.0 broadcast_in_dim.39
  312.5 3.5 all-to-all-start.3
  316.1 4.1 %collective-permute-start = (f32[2,256]{1,0:T(2,128)S(1)}, f32[2,256]{1,0:T(2,128)S(1)}, u32[]{:S(2)}, u32[]{:S(2)}) collective-permute-start(f32[2,256]{1,0:T(2,128)S(1)} %slice.57), channel_id=1, source_target_pairs={{0,4},{4,8},{8,12},{12,16},{16,20},{20,24},{24,28},{28,32},{32,36}... | collective-permute-start | bytes 6152 | tf_op jit(solution)/shard_map/ppermute | solution.py:52
  320.3 0.7 collective-permute-done
  321.0 9.1 %all-to-all-done.3 = bf16[4,256,512]{1,2,0:T(8,128)(2,1)S(1)} async-done(((bf16[4,256,512]{1,2,0:T(8,128)(2,1)}), bf16[4,256,512]{1,2,0:T(8,128)(2,1)S(1)}, u32[]{:S(2)}, u32[]{:S(2)}) %all-to-all-start.3) | async-done | bytes 1048608 | tf_op jit(solution)/shard_map/all_to_all | solution.py:42
  330.1 2.4 multiply_convert_fusion.5
  332.4 2.3 convolution_convert_fusion
  334.8 7.4 %all-to-all-start.4 = ((bf16[64,32,256]{2,1,0:T(8,128)(2,1)}), bf16[64,32,256]{2,1,0:T(8,128)(2,1)S(1)}, u32[]{:S(2)}, u32[]{:S(2)}) async-start(bf16[64,32,256]{2,1,0:T(8,128)(2,1)} %bitcast.82), calls=%async_computation.4 | async-start | bytes 2097152 | tf_op jit(solution)/shard_map/all_to_all | solution.py:30
  342.2 4.0 %fusion.3 = bf16[1,2048,256]{2,1,0:T(8,128)(2,1)} fusion(bf16[768,256]{1,0:T(8,128)(2,1)S(1)} %get-tuple-element.15, bf16[2,768,2048]{2,1,0:T(8,128)(2,1)} %all-gather.2.cloned.1.call-done), kind=kOutput, calls=%fused_computation.15 | convolution fusion | flops 805830656 | bytes 4587520 | tf_op jit(solution)/shard_map/erd,erf->edf/dot_general | solution.py:112
  346.2 4.0 %fusion.5 = bf16[1,256,2048]{2,1,0:T(8,128)(2,1)} fusion(bf16[2,768,2048]{2,1,0:T(8,128)(2,1)} %all-gather.2.cloned.1.call-done, f32[768,256]{1,0:T(8,128)S(1)} %copy-done.18, f32[768,256]{1,0:T(8,128)S(1)} %copy-done.16), kind=kOutput, calls=%fused_computation.17 | convolution fusion | flops 807010304 | bytes 5767168 | tf_op jit(solution)/shard_map/erf,erd->efd/dot_general | solution.py:109
  350.2 2.5 collective-permute-start.1
  352.7 3.9 %fusion.4 = bf16[1,2048,256]{2,1,0:T(8,128)(2,1)} fusion(bf16[768,256]{1,0:T(8,128)(2,1)S(1)} %copy-done.9, bf16[2,768,2048]{2,1,0:T(8,128)(2,1)} %all-gather.2.cloned.1.call-done), kind=kOutput, calls=%fused_computation.16 | convolution fusion | flops 805830656 | bytes 4587520 | tf_op jit(solution)/shard_map/erd,erf->edf/dot_general | solution.py:115
  356.7 0.8 fusion.24
  357.4 0.7 fusion.25
  358.1 12.2 %all-to-all-done.4 = bf16[64,32,256]{2,1,0:T(8,128)(2,1)S(1)} async-done(((bf16[64,32,256]{2,1,0:T(8,128)(2,1)}), bf16[64,32,256]{2,1,0:T(8,128)(2,1)S(1)}, u32[]{:S(2)}, u32[]{:S(2)}) %all-to-all-start.4) | async-done | bytes 1048608 | tf_op jit(solution)/shard_map/all_to_all | solution.py:30
  370.4 0.8 convert_reduce_fusion
  (116 shorter events, 33.0 us)
Async XLA Ops:
  7.2 158.2 %copy-start = (bf16[1,2048,256]{2,1,0:T(8,128)(2,1)S(1)}, bf16[1,2048,256]{2,1,0:T(8,128)(2,1)}, u32[]{:S(2)}) copy-start(bf16[1,2048,256]{2,1,0:T(8,128)(2,1)} %param.16) | copy-start | bytes 3145732
  7.2 158.2 %all-gather.2.cloned.1.call-start = ((), (), s32[]{:S(2)}) async-start(), calls=%async_computation.5 | async-start | bytes 7864320 | tf_op jit(solution)/shard_map/all_gather | solution.py:20
  14.5 4.6 %copy-start.11 = (f32[256,2]{0,1:T(2,128)S(1)}, f32[256,2]{0,1:T(2,128)}, u32[]{:S(2)}) copy-start(f32[256,2]{0,1:T(2,128)} %param.15) | copy-start | bytes 6148
  31.0 1.2 copy-start.1
  99.4 69.0 %copy-start.3 = (bf16[1,2048,256]{2,1,0:T(8,128)(2,1)S(1)}, bf16[1,2048,256]{2,1,0:T(8,128)(2,1)}, u32[]{:S(2)}) copy-start(bf16[1,2048,256]{2,1,0:T(8,128)(2,1)} %param.17) | copy-start | bytes 3145732
  165.4 3.7 copy-start.13
  169.1 1.0 copy-start.15
  169.1 1.5 copy-start.14
  170.6 1.2 copy-start.17
  171.8 1.0 copy-start.8
  266.1 40.1 %all-to-all-start.2 = ((bf16[64,1,12,512]{3,2,1,0:T(8,128)(2,1)}), bf16[64,1,12,512]{3,2,1,0:T(8,128)(2,1)S(1)}, u32[]{:S(2)}, u32[]{:S(2)}) async-start(bf16[64,1,12,512]{3,2,1,0:T(8,128)(2,1)} %constant_dynamic-update-slice_fusion), calls=%async_computation.2 | async-start | bytes 2097152 | tf_op jit(solution)/shard_map/all_to_all | solution.py:125
  309.0 7.0 %copy-start.4 = (bf16[256,256]{1,0:T(8,128)(2,1)S(1)}, bf16[256,256]{1,0:T(8,128)(2,1)}, u32[]{:S(2)}) copy-start(bf16[256,256]{1,0:T(8,128)(2,1)} %param.20) | copy-start | bytes 393220
  309.0 7.0 %copy-start.6 = (bf16[256,256]{1,0:T(8,128)(2,1)S(1)}, bf16[256,256]{1,0:T(8,128)(2,1)}, u32[]{:S(2)}) copy-start(bf16[256,256]{1,0:T(8,128)(2,1)} %param.21) | copy-start | bytes 393220
  310.3 10.0 %copy-start.10 = (bf16[3,256]{1,0:T(4,128)(2,1)S(1)}, bf16[3,256]{1,0:T(4,128)(2,1)}, u32[]{:S(2)}) copy-start(bf16[3,256]{1,0:T(4,128)(2,1)} %param.22) | copy-start | bytes 4612
  311.3 21.1 %copy-start.2 = (bf16[256,512]{1,0:T(8,128)(2,1)}, bf16[256,512]{1,0:T(8,128)(2,1)S(1)}, u32[]{:S(2)}) copy-start(bf16[256,512]{1,0:T(8,128)(2,1)S(1)} %add_convert_fusion.1) | copy-start | bytes 786436
  312.5 17.5 %all-to-all-start.3 = ((bf16[4,256,512]{1,2,0:T(8,128)(2,1)}), bf16[4,256,512]{1,2,0:T(8,128)(2,1)S(1)}, u32[]{:S(2)}, u32[]{:S(2)}) async-start(bf16[4,256,512]{1,2,0:T(8,128)(2,1)} %broadcast_in_dim.39), calls=%async_computation.3 | async-start | bytes 2097152 | tf_op jit(solution)/shard_map/all_to_all | solution.py:42
  316.1 4.9 %collective-permute-start = (f32[2,256]{1,0:T(2,128)S(1)}, f32[2,256]{1,0:T(2,128)S(1)}, u32[]{:S(2)}, u32[]{:S(2)}) collective-permute-start(f32[2,256]{1,0:T(2,128)S(1)} %slice.57), channel_id=1, source_target_pairs={{0,4},{4,8},{8,12},{12,16},{16,20},{20,24},{24,28},{28,32},{32,36}... | collective-permute-start | bytes 6152 | tf_op jit(solution)/shard_map/ppermute | solution.py:52
  321.0 9.1 %copy-start.12 = (f32[2,256]{1,0:T(2,128)}, f32[2,256]{1,0:T(2,128)S(1)}, u32[]{:S(2)}) copy-start(f32[2,256]{1,0:T(2,128)S(1)} %collective-permute-done) | copy-start | bytes 6148
  334.8 35.6 %all-to-all-start.4 = ((bf16[64,32,256]{2,1,0:T(8,128)(2,1)}), bf16[64,32,256]{2,1,0:T(8,128)(2,1)S(1)}, u32[]{:S(2)}, u32[]{:S(2)}) async-start(bf16[64,32,256]{2,1,0:T(8,128)(2,1)} %bitcast.82), calls=%async_computation.4 | async-start | bytes 2097152 | tf_op jit(solution)/shard_map/all_to_all | solution.py:30
  342.2 4.0 %copy-start.16 = (f32[768,256]{1,0:T(8,128)S(1)}, f32[768,256]{1,0:T(8,128)}, u32[]{:S(2)}) copy-start(f32[768,256]{1,0:T(8,128)} %copy-done.15) | copy-start | bytes 2359300
  342.2 4.0 %copy-start.18 = (f32[768,256]{1,0:T(8,128)S(1)}, f32[768,256]{1,0:T(8,128)}, u32[]{:S(2)}) copy-start(f32[768,256]{1,0:T(8,128)} %copy-done.17) | copy-start | bytes 2359300
  346.2 6.5 %copy-start.9 = (bf16[768,256]{1,0:T(8,128)(2,1)S(1)}, bf16[768,256]{1,0:T(8,128)(2,1)}, u32[]{:S(2)}) copy-start(bf16[768,256]{1,0:T(8,128)(2,1)} %copy-done.8) | copy-start | bytes 1179652
  350.2 6.4 %copy-start.5 = (bf16[256,256]{1,0:T(8,128)(2,1)S(1)}, bf16[256,256]{1,0:T(8,128)(2,1)}, u32[]{:S(2)}) copy-start(bf16[256,256]{1,0:T(8,128)(2,1)} %param.20) | copy-start | bytes 393220
  350.2 7.2 %copy-start.7 = (bf16[256,256]{1,0:T(8,128)(2,1)S(1)}, bf16[256,256]{1,0:T(8,128)(2,1)}, u32[]{:S(2)}) copy-start(bf16[256,256]{1,0:T(8,128)(2,1)} %param.21) | copy-start | bytes 393220
  350.2 6.4 %collective-permute-start.1 = (f32[2,256]{1,0:T(2,128)S(1)}, f32[2,256]{1,0:T(2,128)S(1)}, u32[]{:S(2)}, u32[]{:S(2)}) collective-permute-start(f32[2,256]{1,0:T(2,128)S(1)} %slice.62), channel_id=1, source_target_pairs={{4,0},{8,4},{12,8},{16,12},{20,16},{24,20},{28,24},{32,28},{36,32}... | collective-permute-start | bytes 6152 | tf_op jit(solution)/shard_map/ppermute | solution.py:52
Sparse Core Ops, SparseCore 0:
  99.5 65.8 all-gather.1
